TPU v7x, 512 devices: a 4x2x32 block of a 4x8x32 slice. The times are simulated.
512 devices in a mesh: grp: 2 (over y), fs: 32 (over z), tp: 8 (over x, core).
Axes of the slice: x: 4, y: 2, z: 32, core: 2. Of those that a mesh axis runs over, the one named last changes fastest.
The devices are a block of a 4x8x32 slice.
Arguments:
- tokens: bfloat16 [64, 384, 2048], P(('grp', 'fs'), None, 'tp'), parts along dimension 0, may hold values from -24 to 24
- input_gain: float32 [2048], replicated, may hold values from 0.1 to 1.9
- query_weight: bfloat16 [2048, 1024], P('fs', 'tp'), may hold values from -0.125 to 0.125
- key_weight: bfloat16 [2048, 1024], P('fs', 'tp'), may hold values from -0.125 to 0.125
- value_weight: bfloat16 [2048, 1024], P('fs', 'tp'), may hold values from -0.125 to 0.125
- output_gate_matrix: bfloat16 [2048, 1024], P('fs', 'tp'), may hold values from -0.125 to 0.125
- forward_decay: float32 [16], P('tp'), may hold values from -1 to 9
- backward_decay: float32 [16], P('tp'), may hold values from -1 to 9
- merge_weight: bfloat16 [1024, 2048], P('tp', 'fs'), may hold values from -0.375 to 0.375
- middle_gain: float32 [2048], replicated, may hold values from 0.1 to 1.9
- gate_weight: bfloat16 [2048, 5120], P('fs', 'tp'), may hold values from -0.125 to 0.125
- up_weight: bfloat16 [2048, 5120], P('fs', 'tp'), may hold values from -0.125 to 0.125
- down_weight: bfloat16 [5120, 2048], P('tp', 'fs'), may hold values from -0.15625 to 0.15625
Outputs:
- layer_out: bfloat16 [64, 384, 2048], P(('grp', 'fs'), None, 'tp'), parts along dimension 0
There are 2 independent parts, one for each index of `grp`. A program takes and returns all parts, laid end to end along the dimension named above; an argument that names none is the same for every part. Nothing has to cross between parts.
All inputs are finite; a program needn't handle non-finite values.
Results may differ from a plain program's by a relative error of at most 0.019.
Values may be sent and summed in bfloat16 or wider, within the bound.
No kernel may reach another device: no remote copies, remote signals or barrier semaphores. Data moves between devices by JAX's collectives and lax.ppermute only.
A program may use at most 64 MiB of HBM per device.

v0:
```python
import jax
import jax.numpy as jnp
from jax import lax
from jax.experimental import pallas as pl
from jax.experimental.pallas import tpu as pltpu
from jax.sharding import PartitionSpec as P


BLOCK = 128


norm_eps = 1e-06
group_eps = 1e-05
rope_base = 10000.0
highest_precision = lax.Precision.HIGHEST


def core_pairs():
    peers = lax.axis_size("tp")
    return [[i, i + 1] for i in range(0, peers, 2)]


def chip_rings():
    peers = lax.axis_size("tp")
    return [list(range(0, peers, 2)), list(range(1, peers, 2))]


def gathered_features(shard):
    chips = lax.all_gather(shard, "tp", axis=0, axis_index_groups=chip_rings())
    both = jnp.broadcast_to(chips, (2, *chips.shape))
    both = lax.all_to_all(both, "tp", 0, 0, tiled=True, axis_index_groups=core_pairs())
    return jnp.concatenate(
        [both[c, x] for x in range(chips.shape[0]) for c in range(2)], axis=1
    )


def by_core_and_chip(partial_term):
    peers = lax.axis_size("tp")
    width = partial_term.shape[1] // peers
    parts = [partial_term[:, t * width : (t + 1) * width] for t in range(peers)]
    return jnp.stack([jnp.stack(parts[0::2]), jnp.stack(parts[1::2])])


def scattered_sum(tiles):
    tiles = lax.all_to_all(tiles, "tp", 0, 0, tiled=True, axis_index_groups=core_pairs())
    chip_sum = (tiles[0].astype(jnp.float32) + tiles[1].astype(jnp.float32)).astype(jnp.bfloat16)
    tiles = lax.all_to_all(chip_sum, "tp", 0, 0, tiled=True, axis_index_groups=chip_rings())
    return jnp.sum(tiles.astype(jnp.float32), axis=0)


def group_pairs():
    return [(i, i ^ 1) for i in range(lax.axis_size("grp"))]


def parity_rings():
    peers = lax.axis_size("fs")
    return [list(range(0, peers, 2)), list(range(1, peers, 2))]


def from_neighbours(ring):
    peers = lax.axis_size("fs")
    half = ring.shape[0] // 2
    upper = lax.ppermute(ring[:half], "fs", [(i, (i - 1) % peers) for i in range(peers)])
    lower = lax.ppermute(ring[half:], "fs", [(i, (i + 1) % peers) for i in range(peers)])
    return jnp.concatenate([upper, lower], axis=0)


def in_order(own, other, block):
    first = lax.axis_index("fs") % 2 == 0
    own = own.reshape(-1, block, own.shape[1])
    other = other.reshape(own.shape)
    both = jnp.stack([jnp.where(first, own, other), jnp.where(first, other, own)], axis=1)
    return both.reshape(-1, own.shape[2])


def gathered_by_pairs(left, right, common):
    paired = lax.axis_size("grp") % 2 == 0
    block, width = left.shape
    if not paired:
        rows = []
        for piece in (left, right, common):
            ring = lax.all_gather(piece, "fs", axis=0, tiled=True, axis_index_groups=parity_rings())
            rows.append(in_order(ring, from_neighbours(ring), block))
        return rows
    lower = lax.axis_index("grp") % 2 == 0
    mine = jnp.concatenate([jnp.where(lower, left, right), common], axis=1)
    ring = lax.all_gather(mine, "fs", axis=0, tiled=True, axis_index_groups=parity_rings())
    near = from_neighbours(ring)
    ring_pair = lax.ppermute(ring[:, :width], "grp", group_pairs())
    near_pair = lax.ppermute(near[:, :width], "grp", group_pairs())
    mine = in_order(ring, near, block)
    theirs = in_order(ring_pair, near_pair, block)
    return mine[:, :width], theirs, mine[:, width:]


def rms_scale(values, gain_vector):
    widened = values.astype(jnp.float32)
    scaled = widened * lax.rsqrt(jnp.mean(widened * widened, axis=-1, keepdims=True) + norm_eps)
    return (scaled * gain_vector).astype(jnp.bfloat16)


def apply_rotary_heads(values, length):
    half_dim = values.shape[-1] // 2
    inverse = rope_base ** (-jnp.arange(half_dim, dtype=jnp.float32) / half_dim)
    angles = jnp.arange(length, dtype=jnp.float32)[:, None] * inverse[None, :]
    cosine = jnp.cos(angles)[:, None, :]
    sine_part = jnp.sin(angles)[:, None, :]
    lower_half = values[..., :half_dim]
    upper_half = values[..., half_dim:]
    return jnp.concatenate(
        [
            lower_half * cosine - upper_half * sine_part,
            upper_half * cosine + lower_half * sine_part,
        ],
        axis=-1,
    )


def carry_states(key_blocks, value_blocks, weighting, log_rates, block_size, backward):
    block_terms = jnp.einsum(
        "sbmhd,sbmhe->bshde",
        key_blocks * weighting[None, None, :, :, None],
        value_blocks,
        precision=highest_precision,
    )
    factor = jnp.exp(log_rates * block_size)[None, :, None, None]

    def advance(running, addend):
        return (running * factor + addend, running)

    initial = jnp.zeros(block_terms.shape[1:], jnp.float32)
    return lax.scan(advance, initial, block_terms, reverse=backward)[1]


def retain_blocks(
    query_rows, key_rows, value_rows, gate_rows, forward_decay, backward_decay, seq_count, length
):
    head_count = forward_decay.shape[0]
    head_dim = query_rows.shape[1] // head_count
    block_size = BLOCK
    block_count = length // block_size

    def split_heads(rows_in):
        return rows_in.astype(jnp.float32).reshape(seq_count, length, head_count, head_dim)

    def blocked(tensor):
        return tensor.reshape(seq_count, block_count, block_size, head_count, head_dim)

    queries = blocked(apply_rotary_heads(split_heads(query_rows), length))
    key_heads = blocked(apply_rotary_heads(split_heads(key_rows), length) * head_dim ** (-0.5))
    valued = blocked(split_heads(value_rows))
    rate_ahead = jax.nn.log_sigmoid(forward_decay)
    rate_behind = jax.nn.log_sigmoid(backward_decay)
    position = jnp.arange(block_size, dtype=jnp.float32)
    offset = position[:, None] - position[None, :]
    inside = jnp.where(
        offset[None] >= 0,
        jnp.exp(rate_ahead[:, None, None] * jnp.maximum(offset, 0.0)[None]),
        jnp.exp(rate_behind[:, None, None] * jnp.maximum(-offset, 0.0)[None]),
    )
    attention_scores = (
        jnp.einsum("sbchd,sbmhd->sbhcm", queries, key_heads, precision=highest_precision)
        * inside[None, None]
    )
    result = jnp.einsum("sbhcm,sbmhd->sbchd", attention_scores, valued, precision=highest_precision)
    column = position[:, None]
    key_ahead = jnp.exp(rate_ahead[None, :] * (block_size - 1 - column))
    query_ahead = jnp.exp(rate_ahead[None, :] * (column + 1))
    key_behind = jnp.exp(rate_behind[None, :] * column)
    query_behind = jnp.exp(rate_behind[None, :] * (block_size - column))
    from_before = carry_states(key_heads, valued, key_ahead, rate_ahead, block_size, False)
    from_after = carry_states(key_heads, valued, key_behind, rate_behind, block_size, True)
    result = (
        result
        + jnp.einsum("sbchd,bshde->sbche", queries, from_before, precision=highest_precision)
        * query_ahead[None, None, :, :, None]
    )
    result = (
        result
        + jnp.einsum("sbchd,bshde->sbche", queries, from_after, precision=highest_precision)
        * query_behind[None, None, :, :, None]
    )
    result = result.reshape(seq_count, length, head_count, head_dim)
    center = jnp.mean(result, axis=-1, keepdims=True)
    spread = jnp.mean(jnp.square(result - center), axis=-1, keepdims=True)
    normalized = (result - center) * lax.rsqrt(spread + group_eps)
    gated = jax.nn.silu(split_heads(gate_rows)) * normalized
    return gated.reshape(seq_count * length, head_count * head_dim).astype(jnp.bfloat16)


def feed_forward_kernel(
    normed_ref, packed_ref, out_ref, upper_ref, down_ref, acts_ref, upper_sem, down_sem
):
    units = down_ref.shape[1]
    blocks, depth = upper_ref.shape[0], upper_ref.shape[1]
    width = out_ref.shape[2]
    peers = out_ref.shape[0] * out_ref.shape[1]
    upper, down = [], []
    for k in range(blocks):
        rows = pl.ds(k * depth, depth)
        source = packed_ref.at[rows, pl.ds(0, 2 * units)]
        upper.append(pltpu.make_async_copy(source, upper_ref.at[k], upper_sem.at[k]))
    for k in range(blocks):
        rows = pl.ds(k * depth, depth)
        source = packed_ref.at[rows, pl.ds(2 * units, units)]
        down.append(pltpu.make_async_copy(source, down_ref.at[rows], down_sem.at[k]))
    for copy in upper + down:
        copy.start()
    for k in range(blocks):
        upper[k].wait()
        term = jnp.dot(
            normed_ref[:, k * depth : (k + 1) * depth],
            upper_ref[k],
            preferred_element_type=jnp.float32,
        )
        if k == 0:
            acts_ref[...] = term
        else:
            acts_ref[...] += term
    gate_act, up_act = acts_ref[:, :units], acts_ref[:, units:]
    hidden = gate_act / (1.0 + jnp.exp(-gate_act)) * up_act
    hidden = hidden.T.astype(jnp.bfloat16)
    for k in range(blocks):
        down[k].wait()
    for t in range(peers):
        term = jnp.dot(
            down_ref[t * width : (t + 1) * width], hidden, preferred_element_type=jnp.float32
        )
        out_ref[t % 2, t // 2] = term.astype(out_ref.dtype)


def feed_forward(normed_mid, packed, peers):
    rows, features = normed_mid.shape
    units = packed.shape[1] // 3
    width, depth = features // peers, 512
    blocks = features // depth
    return pl.pallas_call(
        feed_forward_kernel,
        out_shape=jax.ShapeDtypeStruct((2, peers // 2, width, rows), jnp.bfloat16),
        in_specs=[
            pl.BlockSpec(memory_space=pltpu.VMEM),
            pl.BlockSpec(memory_space=pltpu.HBM),
        ],
        out_specs=pl.BlockSpec(memory_space=pltpu.VMEM),
        scratch_shapes=[
            pltpu.VMEM((blocks, depth, 2 * units), jnp.bfloat16),
            pltpu.VMEM((features, units), jnp.bfloat16),
            pltpu.VMEM((rows, 2 * units), jnp.float32),
            pltpu.SemaphoreType.DMA((blocks,)),
            pltpu.SemaphoreType.DMA((blocks,)),
        ],
        compiler_params=pltpu.CompilerParams(vmem_limit_bytes=57 * 1024 * 1024),
    )(normed_mid, packed)


def on_device(
    tokens,
    input_gain,
    query_weight,
    key_weight,
    value_weight,
    output_gate_matrix,
    forward_decay,
    backward_decay,
    merge_weight,
    middle_gain,
    gate_weight,
    up_weight,
    down_weight,
):
    seq_count, length, part_width = tokens.shape
    row_count = seq_count * length
    packed = jnp.concatenate([gate_weight, up_weight, down_weight.T], axis=1)
    packed = lax.all_gather(packed, "fs", axis=0, tiled=True)

    mine_full, theirs_full, merge_full = gathered_by_pairs(
        jnp.concatenate([query_weight, key_weight], axis=1),
        jnp.concatenate([value_weight, output_gate_matrix], axis=1),
        merge_weight.T,
    )
    local = tokens.reshape(row_count, part_width)
    gathered = gathered_features(local)
    normed = rms_scale(gathered, input_gain)

    def project(weight):
        return jnp.dot(normed, weight, preferred_element_type=jnp.float32).astype(jnp.bfloat16)

    mine_rows, theirs_rows = project(mine_full), project(theirs_full)
    lower = lax.axis_index("grp") % 2 == 0
    lower = jnp.logical_or(lower, lax.axis_size("grp") % 2 == 1)
    left_rows = jnp.where(lower, mine_rows, theirs_rows)
    right_rows = jnp.where(lower, theirs_rows, mine_rows)
    head_width = query_weight.shape[1]
    mixed = retain_blocks(
        left_rows[:, :head_width],
        left_rows[:, head_width:],
        right_rows[:, :head_width],
        right_rows[:, head_width:],
        forward_decay,
        backward_decay,
        seq_count,
        length,
    )
    merge_term = jnp.einsum("rh,dh->rd", mixed, merge_full, preferred_element_type=jnp.float32)
    merged = scattered_sum(by_core_and_chip(merge_term.astype(jnp.bfloat16)))
    middle = (local.astype(jnp.float32) + merged).astype(jnp.bfloat16)
    normed_mid = rms_scale(gathered_features(middle), middle_gain)
    summed = scattered_sum(feed_forward(normed_mid, packed, lax.axis_size("tp"))).T
    layer_out = (middle.astype(jnp.float32) + summed).astype(jnp.bfloat16)
    return layer_out.reshape(seq_count, length, part_width)


def solution(mesh):
    placed = (
        P(("grp", "fs"), None, "tp"),
        P(),
        P("fs", "tp"),
        P("fs", "tp"),
        P("fs", "tp"),
        P("fs", "tp"),
        P("tp"),
        P("tp"),
        P("tp", "fs"),
        P(),
        P("fs", "tp"),
        P("fs", "tp"),
        P("tp", "fs"),
    )

    return jax.shard_map(
        on_device,
        mesh=mesh,
        in_specs=placed,
        out_specs=P(("grp", "fs"), None, "tp"),
        check_vma=False,
    )
```

profile of v0, /device:TPU:33, one launch (start us, length us, event | category | flops | bytes accessed | tf_op | source)
XLA Modules:
  0.0 301.2 jit_solution(2100616126508262297)
XLA Ops:
  6.5 0.8 maximum_select_fusion
  7.4 0.7 pad_maximum_fusion.5
  8.1 74.5 %all_gather.14 = bf16[1024,384]{1,0:T(8,128)(2,1)S(1)} all-gather(bf16[64,384]{1,0:T(8,128)(2,1)S(1)} %pad_maximum_fusion.5), channel_id=1, replica_groups={{0,16,32,48,64,80,96,112,128,144,160,176,192,208,224,240},{8,24,40,56,7..., dimensions={0}, use_global_device_ids=true | all-gather | bytes 835584 | tf_op jit(solution)/shard_map/all_gather | solution.py:87
  82.6 1.0 fusion.67
  83.6 3.5 %collective-permute-start.1 = (bf16[512,384]{1,0:T(8,128)(2,1)}, bf16[512,384]{1,0:T(8,128)(2,1)}, u32[]{:S(2)}, u32[]{:S(2)}) collective-permute-start(bf16[512,384]{1,0:T(8,128)(2,1)} %get-tuple-element.260), channel_id=1, source_target_pairs={{0,248},{8,0},{16,8},{24,16},{32,24},{40,32},{48,40},{56,48},{64,5... | collective-permute-start | bytes 1179656 | tf_op jit(solution)/shard_map/ppermute | solution.py:63
  87.1 2.0 collective-permute-start.2
  89.0 10.9 %all_gather.13 = bf16[4,384,256]{2,1,0:T(8,128)(2,1)S(1)} all-gather(bf16[1,384,256]{2,1,0:T(8,128)(2,1)S(1)} %copy-done.2), channel_id=1, replica_groups={{0,2,4,6},{1,3,5,7},{8,10,12,14},{9,11,13,15},{16,18,20,22},{17,19,21,2..., dimensions={0}, use_global_device_ids=true | all-gather | bytes 983040 | tf_op jit(solution)/shard_map/all_gather | solution.py:29
  99.9 1.3 broadcast_in_dim.28
  101.3 15.4 %all-to-all-start = ((bf16[2,4,384,256]{3,2,1,0:T(8,128)(2,1)}), bf16[2,4,384,256]{3,2,1,0:T(8,128)(2,1)S(1)}, u32[]{:S(2)}, u32[]{:S(2)}) async-start(bf16[2,4,384,256]{3,2,1,0:T(8,128)(2,1)} %broadcast_in_dim.28), calls=%async_computation | async-start | bytes 3145728 | tf_op jit(solution)/shard_map/all_to_all | solution.py:31
  116.6 0.8 slice.176
  117.5 3.5 %collective-permute-start = (bf16[1024,256]{1,0:T(8,128)(2,1)}, bf16[1024,256]{1,0:T(8,128)(2,1)S(1)}, u32[]{:S(2)}, u32[]{:S(2)}) collective-permute-start(bf16[1024,256]{1,0:T(8,128)(2,1)} %slice.176), channel_id=1, source_target_pairs={{0,256},{256,0},{1,257},{257,1},{2,258},{258,2},{3,259},{259,3},{4... | collective-permute-start | bytes 1572872 | tf_op jit(solution)/shard_map/ppermute | solution.py:89
  121.1 0.7 pad_maximum_fusion.3
  122.1 1.2 copy-done
  123.4 0.4 fusion
  123.8 0.6 multiply_exponential_fusion
  124.4 0.7 multiply_exponential_fusion.1
  125.0 0.9 fusion.57
  126.2 1.0 constant_dynamic-update-slice_fusion.1
  127.2 1.1 constant_dynamic-update-slice_fusion
  128.3 2.0 collective-permute-start.3
  130.7 1.2 copy-done.1
  131.9 0.9 convolution_convert_fusion.1
  132.8 0.5 collective-permute-done
  133.3 11.3 %collective-permute-done.3 = bf16[1024,256]{1,0:T(8,128)(2,1)S(1)} collective-permute-done((bf16[1024,256]{1,0:T(8,128)(2,1)S(1)}, bf16[1024,256]{1,0:T(8,128)(2,1)S(1)}, u32[]{:S(2)}, u32[]{:S(2)}) %collective-permute-start.3) | collective-permute-done | bytes 524320 | tf_op jit(solution)/shard_map/ppermute | solution.py:90
  144.8 0.9 broadcast_select_fusion.5
  146.2 0.3 copy-done.10
  146.5 0.3 convolution_bitcast_fusion.4
  146.8 0.3 convolution_bitcast_fusion.3
  147.1 0.3 while.30
  147.4 0.5 fusion.8
  147.9 0.3 while.31
  148.2 0.5 fusion.9
  148.7 0.8 convolution_multiply_fusion
  149.5 0.5 fusion.69
  150.3 0.6 convolution_convert_fusion
  151.4 5.3 %all_to_all.30 = bf16[2,4,384,256]{3,2,1,0:T(8,128)(2,1)S(1)} all-to-all(bf16[2,4,384,256]{3,2,1,0:T(8,128)(2,1)S(1)} %pad_maximum_fusion.1), channel_id=1, replica_groups={{0,1},{2,3},{4,5},{6,7},{8,9},{10,11},{12,13},{14,15},{16,17},{18,19},{..., dimensions={0} | all-to-all | bytes 3145728 | tf_op jit(solution)/shard_map/all_to_all | solution.py:45
  156.9 14.8 %all_to_all.31 = bf16[4,384,256]{2,1,0:T(8,128)(2,1)S(1)} all-to-all(bf16[4,384,256]{2,1,0:T(8,128)(2,1)S(1)} %fusion.11), channel_id=1, replica_groups={{0,2,4,6},{1,3,5,7},{8,10,12,14},{9,11,13,15},{16,18,20,22},{17,19,21,2..., dimensions={0} | all-to-all | bytes 1572864 | tf_op jit(solution)/shard_map/all_to_all | solution.py:47
  171.9 12.0 %all_gather.15 = bf16[4,384,256]{2,1,0:T(8,128)(2,1)S(1)} all-gather(bf16[1,384,256]{2,1,0:T(8,128)(2,1)S(1)} %fusion.18), channel_id=1, replica_groups={{0,2,4,6},{1,3,5,7},{8,10,12,14},{9,11,13,15},{16,18,20,22},{17,19,21,2..., dimensions={0}, use_global_device_ids=true | all-gather | bytes 983040 | tf_op jit(solution)/shard_map/all_gather | solution.py:29
  184.0 8.7 %all_to_all.32 = bf16[2,4,384,256]{3,2,1,0:T(8,128)(2,1)S(1)} all-to-all(bf16[2,4,384,256]{3,2,1,0:T(8,128)(2,1)S(1)} %broadcast_in_dim.33), channel_id=1, replica_groups={{0,1},{2,3},{4,5},{6,7},{8,9},{10,11},{12,13},{14,15},{16,17},{18,19},{..., dimensions={0} | all-to-all | bytes 3145728 | tf_op jit(solution)/shard_map/all_to_all | solution.py:31
  193.0 0.4 fusion.3
  193.4 0.2 copy-done.8
  193.6 1.7 fusion.5.normed_ref
  195.2 47.3 %all-gather.2.cloned.1.call-done.packed_ref = bf16[2048,1920]{1,0:T(8,128)(2,1)} async-done(((bf16[64,1920]{1,0:T(8,128)(2,1)}), bf16[2048,1920]{1,0:T(8,128)(2,1)}) %all-gather.2.cloned.1.call-update) | async-done | bytes 7864336 | tf_op jit(solution)/shard_map/all_gather | solution.py:274
  242.6 8.9 %shard_map.127 = bf16[2,4,256,384]{3,2,1,0:T(8,128)(2,1)} custom-call(bf16[384,2048]{1,0:T(8,128)(2,1)} %fusion.5.normed_ref, bf16[2048,1920]{1,0:T(8,128)(2,1)} %all-gather.2.cloned.1.call-done.packed_ref), custom_call_target="tpu_custom_call" | custom-call | tf_op jit(solution)/shard_map/pallas_call | solution.py:237
  251.4 26.5 %all_to_all.33 = bf16[2,4,256,384]{3,2,1,0:T(8,128)(2,1)S(1)} all-to-all(bf16[2,4,256,384]{3,2,1,0:T(8,128)(2,1)} %shard_map.127), channel_id=1, replica_groups={{0,1},{2,3},{4,5},{6,7},{8,9},{10,11},{12,13},{14,15},{16,17},{18,19},{..., dimensions={0} | all-to-all | bytes 3145728 | tf_op jit(solution)/shard_map/all_to_all | solution.py:45
  277.9 0.2 fusion.12
  278.1 15.2 %all_to_all.34 = bf16[4,256,384]{2,1,0:T(8,128)(2,1)S(1)} all-to-all(bf16[4,256,384]{2,1,0:T(8,128)(2,1)S(1)} %fusion.12), channel_id=1, replica_groups={{0,2,4,6},{1,3,5,7},{8,10,12,14},{9,11,13,15},{16,18,20,22},{17,19,21,2..., dimensions={0} | all-to-all | bytes 1572864 | tf_op jit(solution)/shard_map/all_to_all | solution.py:47
  293.6 0.7 fusion.24
  (102 shorter events, 3.5 us)
Async XLA Ops:
  6.5 82.5 %copy-start.2 = (bf16[1,384,256]{2,1,0:T(8,128)(2,1)S(1)}, bf16[1,384,256]{2,1,0:T(8,128)(2,1)}, u32[]{:S(2)}) copy-start(bf16[1,384,256]{2,1,0:T(8,128)(2,1)} %param.17) | copy-start | bytes 589828
  83.6 42.6 %collective-permute-start.1 = (bf16[512,384]{1,0:T(8,128)(2,1)}, bf16[512,384]{1,0:T(8,128)(2,1)}, u32[]{:S(2)}, u32[]{:S(2)}) collective-permute-start(bf16[512,384]{1,0:T(8,128)(2,1)} %get-tuple-element.260), channel_id=1, source_target_pairs={{0,248},{8,0},{16,8},{24,16},{32,24},{40,32},{48,40},{56,48},{64,5... | collective-permute-start | bytes 1179656 | tf_op jit(solution)/shard_map/ppermute | solution.py:63
  87.1 40.2 %collective-permute-start.2 = (bf16[512,384]{1,0:T(8,128)(2,1)}, bf16[512,384]{1,0:T(8,128)(2,1)}, u32[]{:S(2)}, u32[]{:S(2)}) collective-permute-start(bf16[512,384]{1,0:T(8,128)(2,1)} %get-tuple-element.259), channel_id=1, source_target_pairs={{0,8},{8,16},{16,24},{24,32},{32,40},{40,48},{48,56},{56,64},{64,7... | collective-permute-start | bytes 1179656 | tf_op jit(solution)/shard_map/ppermute | solution.py:64
  101.2 19.8 %copy-start.5 = (bf16[640,64]{0,1:T(8,128)(2,1)S(1)}, bf16[640,64]{0,1:T(8,128)(2,1)}, u32[]{:S(2)}) copy-start(bf16[640,64]{0,1:T(8,128)(2,1)} %param.29) | copy-start | bytes 245764
  101.3 19.8 %copy-start.6 = (bf16[64,640]{1,0:T(8,128)(2,1)S(1)}, bf16[64,640]{1,0:T(8,128)(2,1)}, u32[]{:S(2)}) copy-start(bf16[64,640]{1,0:T(8,128)(2,1)} %param.28) | copy-start | bytes 245764
  101.3 19.8 %copy-start.7 = (bf16[64,640]{1,0:T(8,128)(2,1)S(1)}, bf16[64,640]{1,0:T(8,128)(2,1)}, u32[]{:S(2)}) copy-start(bf16[64,640]{1,0:T(8,128)(2,1)} %param.27) | copy-start | bytes 245764
  101.3 20.6 %all-to-all-start = ((bf16[2,4,384,256]{3,2,1,0:T(8,128)(2,1)}), bf16[2,4,384,256]{3,2,1,0:T(8,128)(2,1)S(1)}, u32[]{:S(2)}, u32[]{:S(2)}) async-start(bf16[2,4,384,256]{3,2,1,0:T(8,128)(2,1)} %broadcast_in_dim.28), calls=%async_computation | async-start | bytes 3145728 | tf_op jit(solution)/shard_map/all_to_all | solution.py:31
  116.6 125.9 %all-gather.2.cloned.1.call-start = ((), (), s32[]{:S(2)}) async-start(), calls=%async_computation.6 | async-start | bytes 8110080 | tf_op jit(solution)/shard_map/all_gather | solution.py:274
  117.5 15.8 %collective-permute-start = (bf16[1024,256]{1,0:T(8,128)(2,1)}, bf16[1024,256]{1,0:T(8,128)(2,1)S(1)}, u32[]{:S(2)}, u32[]{:S(2)}) collective-permute-start(bf16[1024,256]{1,0:T(8,128)(2,1)} %slice.176), channel_id=1, source_target_pairs={{0,256},{256,0},{1,257},{257,1},{2,258},{258,2},{3,259},{259,3},{4... | collective-permute-start | bytes 1572872 | tf_op jit(solution)/shard_map/ppermute | solution.py:89
  122.0 1.8 copy-start.11
  122.0 1.8 copy-start.12
  122.1 1.3 copy-start
  128.3 16.3 %collective-permute-start.3 = (bf16[1024,256]{1,0:T(8,128)(2,1)S(1)}, bf16[1024,256]{1,0:T(8,128)(2,1)S(1)}, u32[]{:S(2)}, u32[]{:S(2)}) collective-permute-start(bf16[1024,256]{1,0:T(8,128)(2,1)S(1)} %slice.179), channel_id=1, source_target_pairs={{0,256},{256,0},{1,257},{257,1},{2,258},{258,2},{3,259},{259,3},{4... | collective-permute-start | bytes 1572872 | tf_op jit(solution)/shard_map/ppermute | solution.py:90
  130.5 1.4 copy-start.1
  130.5 1.4 copy-start.13
  144.8 1.0 copy-start.3
  144.8 1.0 copy-start.4
  145.8 0.7 copy-start.10
  145.8 0.9 copy-start.9
  192.8 0.7 copy-start.8
Sparse Core Ops, SparseCore 0:
  121.9 120.5 all-gather.1
where the time goes:
time: 302 us; the launch traced here: 301 us
  blocking collectives  168 us (56%)
  waiting for transfers between devices  59.3 us (20%)
  starting transfers between devices  26.3 us (9%)
  between operations  14.1 us (5%)
  other arithmetic  10.1 us (3%)
  local copies, waits for them, and re-layouts  9.35 us (3%)
  Pallas kernels  8.87 us (3%)
  matrix products  5.22 us (2%)
    all_gather x1, blocking collectives, gathered_by_pairs(): lax.all_gather(mine, 'fs', axis=0, tiled=True, axis_index_groups=parity_r...  74.5 us
    all_gather x1, waiting for transfers between devices, on_device(): packed = lax.all_gather(packed, 'fs', axis=0, tiled=True)  47.3 us
    all_to_all x2, blocking collectives, scattered_sum(): lax.all_to_all(tiles, 'tp', 0, 0, tiled=True, axis_index_groups=core_pair...  31.8 us
    all_to_all x2, blocking collectives, scattered_sum(): lax.all_to_all(chip_sum, 'tp', 0, 0, tiled=True, axis_index_groups=chip_r...  30 us
    all_gather x2, blocking collectives, gathered_features(): chips = lax.all_gather(shard, 'tp', axis=0, axis_index_groups=chip_rings())  22.9 us
    all_to_all x1, starting transfers between devices, gathered_features(): lax.all_to_all(both, 'tp', 0, 0, tiled=True, axis_index_groups=core_pairs())  15.4 us
    ppermute x1, waiting for transfers between devices, gathered_by_pairs(): near_pair = lax.ppermute(near[:, :width], 'grp', group_pairs())  11.3 us
    pallas_call x1, Pallas kernels, feed_forward(): pl.pallas_call(feed_forward_kernel, out_shape=jax.ShapeDtypeStruct((2, pe...  8.87 us
  transfers between devices with their start and end apart: 6, of which 3 were waited for; matrix products, arithmetic and copies ran while one was open for 6% of the time, Pallas kernels for 0%

commit v1 on v0

--- a/solution.py
+++ b/solution.py
@@ -85,9 +85,9 @@
     lower = lax.axis_index("grp") % 2 == 0
     mine = jnp.concatenate([jnp.where(lower, left, right), common], axis=1)
     ring = lax.all_gather(mine, "fs", axis=0, tiled=True, axis_index_groups=parity_rings())
+    ring_pair = lax.ppermute(ring[:, :width], "grp", group_pairs())
     near = from_neighbours(ring)
-    ring_pair = lax.ppermute(ring[:, :width], "grp", group_pairs())
-    near_pair = lax.ppermute(near[:, :width], "grp", group_pairs())
+    near_pair = from_neighbours(ring_pair)
     mine = in_order(ring, near, block)
     theirs = in_order(ring_pair, near_pair, block)
     return mine[:, :width], theirs, mine[:, width:]
@@ -193,7 +193,7 @@
 ):
     units = down_ref.shape[1]
     blocks, depth = upper_ref.shape[0], upper_ref.shape[1]
-    width = out_ref.shape[2]
+    width = out_ref.shape[3]
     peers = out_ref.shape[0] * out_ref.shape[1]
     upper, down = [], []
     for k in range(blocks):
@@ -218,13 +218,15 @@
         else:
             acts_ref[...] += term
     gate_act, up_act = acts_ref[:, :units], acts_ref[:, units:]
-    hidden = gate_act / (1.0 + jnp.exp(-gate_act)) * up_act
-    hidden = hidden.T.astype(jnp.bfloat16)
+    hidden = (gate_act / (1.0 + jnp.exp(-gate_act)) * up_act).astype(jnp.bfloat16)
     for k in range(blocks):
         down[k].wait()
     for t in range(peers):
-        term = jnp.dot(
-            down_ref[t * width : (t + 1) * width], hidden, preferred_element_type=jnp.float32
+        term = lax.dot_general(
+            hidden,
+            down_ref[t * width : (t + 1) * width],
+            (((1,), (1,)), ((), ())),
+            preferred_element_type=jnp.float32,
         )
         out_ref[t % 2, t // 2] = term.astype(out_ref.dtype)
 
@@ -236,7 +238,7 @@
     blocks = features // depth
     return pl.pallas_call(
         feed_forward_kernel,
-        out_shape=jax.ShapeDtypeStruct((2, peers // 2, width, rows), jnp.bfloat16),
+        out_shape=jax.ShapeDtypeStruct((2, peers // 2, rows, width), jnp.bfloat16),
         in_specs=[
             pl.BlockSpec(memory_space=pltpu.VMEM),
             pl.BlockSpec(memory_space=pltpu.HBM),
@@ -279,8 +281,7 @@
         merge_weight.T,
     )
     local = tokens.reshape(row_count, part_width)
-    gathered = gathered_features(local)
-    normed = rms_scale(gathered, input_gain)
+    normed = rms_scale(gathered_features(local), input_gain)
 
     def project(weight):
         return jnp.dot(normed, weight, preferred_element_type=jnp.float32).astype(jnp.bfloat16)
@@ -305,7 +306,7 @@
     merged = scattered_sum(by_core_and_chip(merge_term.astype(jnp.bfloat16)))
     middle = (local.astype(jnp.float32) + merged).astype(jnp.bfloat16)
     normed_mid = rms_scale(gathered_features(middle), middle_gain)
-    summed = scattered_sum(feed_forward(normed_mid, packed, lax.axis_size("tp"))).T
+    summed = scattered_sum(feed_forward(normed_mid, packed, lax.axis_size("tp")))
     layer_out = (middle.astype(jnp.float32) + summed).astype(jnp.bfloat16)
     return layer_out.reshape(seq_count, length, part_width)
 

time: 302 us -> 302 us (level)
  waiting for transfers between devices: 59.3 us -> 54.1 us
  starting transfers between devices: 26.3 us -> 30 us
    ppermute x1 -> x0, waiting for transfers between devices: 11.3 us -> none  [gathered_by_pairs(): near_pair = lax.ppermute(near[:, :width], 'grp', group_pairs())]
    all_gather x1, waiting for transfers between devices: 47.3 us -> 37.1 us  [on_device(): packed = lax.all_gather(packed, 'fs', axis=0, tiled=True)]
    ppermute x1 -> x2, waiting for transfers between devices: 0.01 us -> 7.49 us  [from_neighbours(): lax.ppermute(ring[:half], 'fs', [(i, (i - 1) % peers) for i in range(peer...]
    ppermute x1 -> x2, waiting for transfers between devices: 0.01 us -> 4.9 us  [from_neighbours(): lax.ppermute(ring[half:], 'fs', [(i, (i + 1) % peers) for i in range(peer...]
    ppermute x1, waiting for transfers between devices: 0.53 us -> 4.58 us  [gathered_by_pairs(): ring_pair = lax.ppermute(ring[:, :width], 'grp', group_pairs())]
    ppermute x1 -> x2, starting transfers between devices: 3.49 us -> 6.63 us  [from_neighbours(): lax.ppermute(ring[:half], 'fs', [(i, (i - 1) % peers) for i in range(peer...]
  transfers between devices with their start and end apart: 6 -> 7, of which waited for: 3 -> 4; matrix products, arithmetic and copies ran while one was open for 6% -> 6% of each run, Pallas kernels for 0% -> 0%
where the time goes in v1:
time: 302 us; the launch traced here: 301 us
  blocking collectives  169 us (56%)
  waiting for transfers between devices  54.1 us (18%)
  starting transfers between devices  30 us (10%)
  between operations  14.2 us (5%)
  other arithmetic  10.1 us (3%)
  local copies, waits for them, and re-layouts  8.58 us (3%)
  Pallas kernels  8.4 us (3%)
  matrix products  5.88 us (2%)
    all_gather x1, blocking collectives, gathered_by_pairs(): lax.all_gather(mine, 'fs', axis=0, tiled=True, axis_index_groups=parity_r...  74.5 us
    all_gather x1, waiting for transfers between devices, on_device(): packed = lax.all_gather(packed, 'fs', axis=0, tiled=True)  37.1 us
    all_to_all x2, blocking collectives, scattered_sum(): lax.all_to_all(tiles, 'tp', 0, 0, tiled=True, axis_index_groups=core_pair...  33.1 us
    all_to_all x2, blocking collectives, scattered_sum(): lax.all_to_all(chip_sum, 'tp', 0, 0, tiled=True, axis_index_groups=chip_r...  30.3 us
    all_gather x2, blocking collectives, gathered_features(): chips = lax.all_gather(shard, 'tp', axis=0, axis_index_groups=chip_rings())  22.9 us
    all_to_all x1, starting transfers between devices, gathered_features(): lax.all_to_all(both, 'tp', 0, 0, tiled=True, axis_index_groups=core_pairs())  15.4 us
    all_to_all x1, blocking collectives, gathered_features(): lax.all_to_all(both, 'tp', 0, 0, tiled=True, axis_index_groups=core_pairs())  8.7 us
    pallas_call x1, Pallas kernels, feed_forward(): pl.pallas_call(feed_forward_kernel, out_shape=jax.ShapeDtypeStruct((2, pe...  8.4 us
  transfers between devices with their start and end apart: 7, of which 4 were waited for; matrix products, arithmetic and copies ran while one was open for 6% of the time, Pallas kernels for 0%

profile of v1, /device:TPU:33, one launch (start us, length us, event | category | flops | bytes accessed | tf_op | source)
XLA Modules:
  0.0 300.7 jit_solution(10669276571187491398)
XLA Ops:
  6.5 0.8 maximum_select_fusion
  7.4 0.7 pad_maximum_fusion.5
  8.1 74.5 %all_gather.14 = bf16[1024,384]{1,0:T(8,128)(2,1)S(1)} all-gather(bf16[64,384]{1,0:T(8,128)(2,1)S(1)} %pad_maximum_fusion.5), channel_id=1, replica_groups={{0,16,32,48,64,80,96,112,128,144,160,176,192,208,224,240},{8,24,40,56,7..., dimensions={0}, use_global_device_ids=true | all-gather | bytes 835584 | tf_op jit(solution)/shard_map/all_gather | solution.py:87
  82.6 1.0 fusion.64
  83.6 3.5 %collective-permute-start.3 = (bf16[512,384]{1,0:T(8,128)(2,1)}, bf16[512,384]{1,0:T(8,128)(2,1)}, u32[]{:S(2)}, u32[]{:S(2)}) collective-permute-start(bf16[512,384]{1,0:T(8,128)(2,1)} %get-tuple-element.250), channel_id=1, source_target_pairs={{0,248},{8,0},{16,8},{24,16},{32,24},{40,32},{48,40},{56,48},{64,5... | collective-permute-start | bytes 1179656 | tf_op jit(solution)/shard_map/ppermute | solution.py:63
  87.0 2.0 collective-permute-start.4
  89.0 10.9 %all_gather.13 = bf16[4,384,256]{2,1,0:T(8,128)(2,1)S(1)} all-gather(bf16[1,384,256]{2,1,0:T(8,128)(2,1)S(1)} %copy-done.2), channel_id=1, replica_groups={{0,2,4,6},{1,3,5,7},{8,10,12,14},{9,11,13,15},{16,18,20,22},{17,19,21,2..., dimensions={0}, use_global_device_ids=true | all-gather | bytes 983040 | tf_op jit(solution)/shard_map/all_gather | solution.py:29
  99.9 1.4 broadcast_in_dim.28
  101.3 15.4 %all-to-all-start = ((bf16[2,4,384,256]{3,2,1,0:T(8,128)(2,1)}), bf16[2,4,384,256]{3,2,1,0:T(8,128)(2,1)S(1)}, u32[]{:S(2)}, u32[]{:S(2)}) async-start(bf16[2,4,384,256]{3,2,1,0:T(8,128)(2,1)} %broadcast_in_dim.28), calls=%async_computation | async-start | bytes 3145728 | tf_op jit(solution)/shard_map/all_to_all | solution.py:31
  116.7 0.8 slice.180
  117.5 3.5 %collective-permute-start = (bf16[1024,256]{1,0:T(8,128)(2,1)}, bf16[1024,256]{1,0:T(8,128)(2,1)S(1)}, u32[]{:S(2)}, u32[]{:S(2)}) collective-permute-start(bf16[1024,256]{1,0:T(8,128)(2,1)} %slice.180), channel_id=1, source_target_pairs={{0,256},{256,0},{1,257},{257,1},{2,258},{258,2},{3,259},{259,3},{4... | collective-permute-start | bytes 1572872 | tf_op jit(solution)/shard_map/ppermute | solution.py:88
  121.1 0.7 pad_maximum_fusion.3
  122.1 1.3 copy-done
  123.4 0.4 fusion
  123.8 0.7 multiply_exponential_fusion
  124.5 0.6 multiply_exponential_fusion.1
  125.1 0.9 fusion.54
  126.2 1.0 constant_dynamic-update-slice_fusion.3
  127.3 1.1 constant_dynamic-update-slice_fusion.2
  128.7 4.6 %collective-permute-done = bf16[1024,256]{1,0:T(8,128)(2,1)S(1)} collective-permute-done((bf16[1024,256]{1,0:T(8,128)(2,1)}, bf16[1024,256]{1,0:T(8,128)(2,1)S(1)}, u32[]{:S(2)}, u32[]{:S(2)}) %collective-permute-start) | collective-permute-done | bytes 524320 | tf_op jit(solution)/shard_map/ppermute | solution.py:88
  133.3 3.1 %collective-permute-start.1 = (bf16[512,256]{1,0:T(8,128)(2,1)S(1)}, bf16[512,256]{1,0:T(8,128)(2,1)S(1)}, u32[]{:S(2)}, u32[]{:S(2)}) collective-permute-start(bf16[512,256]{1,0:T(8,128)(2,1)S(1)} %get-tuple-element.252), channel_id=1, source_target_pairs={{0,248},{8,0},{16,8},{24,16},{32,24},{40,32},{48,40},{56,48},{64,5... | collective-permute-start | bytes 786440 | tf_op jit(solution)/shard_map/ppermute | solution.py:63
  136.5 2.5 collective-permute-start.2
  139.0 0.9 convolution_convert_fusion.1
  139.9 7.5 %collective-permute-done.1 = bf16[512,256]{1,0:T(8,128)(2,1)S(1)} collective-permute-done((bf16[512,256]{1,0:T(8,128)(2,1)S(1)}, bf16[512,256]{1,0:T(8,128)(2,1)S(1)}, u32[]{:S(2)}, u32[]{:S(2)}) %collective-permute-start.1) | collective-permute-done | bytes 262176 | tf_op jit(solution)/shard_map/ppermute | solution.py:63
  147.4 4.9 %collective-permute-done.2 = bf16[512,256]{1,0:T(8,128)(2,1)S(1)} collective-permute-done((bf16[512,256]{1,0:T(8,128)(2,1)S(1)}, bf16[512,256]{1,0:T(8,128)(2,1)S(1)}, u32[]{:S(2)}, u32[]{:S(2)}) %collective-permute-start.2) | collective-permute-done | bytes 262176 | tf_op jit(solution)/shard_map/ppermute | solution.py:64
  152.5 0.6 copy-done.11
  153.1 0.9 broadcast_select_fusion.5
  154.4 0.2 copy-done.9
  154.7 0.3 convolution_bitcast_fusion.4
  155.0 0.9 convolution_bitcast_fusion.3
  155.9 0.3 while.30
  156.2 0.5 fusion.8
  156.8 0.3 while.31
  157.1 0.5 fusion.9
  157.6 0.8 convolution_multiply_fusion
  158.4 0.5 fusion.67
  159.2 0.6 convolution_convert_fusion
  160.3 7.0 %all_to_all.30 = bf16[2,4,384,256]{3,2,1,0:T(8,128)(2,1)S(1)} all-to-all(bf16[2,4,384,256]{3,2,1,0:T(8,128)(2,1)S(1)} %pad_maximum_fusion.1), channel_id=1, replica_groups={{0,1},{2,3},{4,5},{6,7},{8,9},{10,11},{12,13},{14,15},{16,17},{18,19},{..., dimensions={0} | all-to-all | bytes 3145728 | tf_op jit(solution)/shard_map/all_to_all | solution.py:45
  167.4 14.7 %all_to_all.31 = bf16[4,384,256]{2,1,0:T(8,128)(2,1)S(1)} all-to-all(bf16[4,384,256]{2,1,0:T(8,128)(2,1)S(1)} %fusion.11), channel_id=1, replica_groups={{0,2,4,6},{1,3,5,7},{8,10,12,14},{9,11,13,15},{16,18,20,22},{17,19,21,2..., dimensions={0} | all-to-all | bytes 1572864 | tf_op jit(solution)/shard_map/all_to_all | solution.py:47
  182.3 12.0 %all_gather.15 = bf16[4,384,256]{2,1,0:T(8,128)(2,1)S(1)} all-gather(bf16[1,384,256]{2,1,0:T(8,128)(2,1)S(1)} %fusion.17), channel_id=1, replica_groups={{0,2,4,6},{1,3,5,7},{8,10,12,14},{9,11,13,15},{16,18,20,22},{17,19,21,2..., dimensions={0}, use_global_device_ids=true | all-gather | bytes 983040 | tf_op jit(solution)/shard_map/all_gather | solution.py:29
  194.4 8.7 %all_to_all.32 = bf16[2,4,384,256]{3,2,1,0:T(8,128)(2,1)S(1)} all-to-all(bf16[2,4,384,256]{3,2,1,0:T(8,128)(2,1)S(1)} %broadcast_in_dim.33), channel_id=1, replica_groups={{0,1},{2,3},{4,5},{6,7},{8,9},{10,11},{12,13},{14,15},{16,17},{18,19},{..., dimensions={0} | all-to-all | bytes 3145728 | tf_op jit(solution)/shard_map/all_to_all | solution.py:31
  203.3 0.4 fusion.3
  203.9 1.7 fusion.5.normed_ref
  205.6 37.1 %all-gather.2.cloned.1.call-done.packed_ref = bf16[2048,1920]{1,0:T(8,128)(2,1)} async-done(((bf16[64,1920]{1,0:T(8,128)(2,1)}), bf16[2048,1920]{1,0:T(8,128)(2,1)}) %all-gather.2.cloned.1.call-update) | async-done | bytes 7864336 | tf_op jit(solution)/shard_map/all_gather | solution.py:276
  242.7 8.4 %shard_map.127 = bf16[2,4,384,256]{3,2,1,0:T(8,128)(2,1)} custom-call(bf16[384,2048]{1,0:T(8,128)(2,1)} %fusion.5.normed_ref, bf16[2048,1920]{1,0:T(8,128)(2,1)} %all-gather.2.cloned.1.call-done.packed_ref), custom_call_target="tpu_custom_call" | custom-call | tf_op jit(solution)/shard_map/pallas_call | solution.py:239
  251.1 26.1 %all_to_all.33 = bf16[2,4,384,256]{3,2,1,0:T(8,128)(2,1)S(1)} all-to-all(bf16[2,4,384,256]{3,2,1,0:T(8,128)(2,1)} %shard_map.127), channel_id=1, replica_groups={{0,1},{2,3},{4,5},{6,7},{8,9},{10,11},{12,13},{14,15},{16,17},{18,19},{..., dimensions={0} | all-to-all | bytes 3145728 | tf_op jit(solution)/shard_map/all_to_all | solution.py:45
  277.4 15.6 %all_to_all.34 = bf16[4,384,256]{2,1,0:T(8,128)(2,1)S(1)} all-to-all(bf16[4,384,256]{2,1,0:T(8,128)(2,1)S(1)} %fusion.12), channel_id=1, replica_groups={{0,2,4,6},{1,3,5,7},{8,10,12,14},{9,11,13,15},{16,18,20,22},{17,19,21,2..., dimensions={0} | all-to-all | bytes 1572864 | tf_op jit(solution)/shard_map/all_to_all | solution.py:47
  293.1 0.7 fusion.16
  (107 shorter events, 3.8 us)
Async XLA Ops:
  6.5 82.5 %copy-start.2 = (bf16[1,384,256]{2,1,0:T(8,128)(2,1)S(1)}, bf16[1,384,256]{2,1,0:T(8,128)(2,1)}, u32[]{:S(2)}) copy-start(bf16[1,384,256]{2,1,0:T(8,128)(2,1)} %param.17) | copy-start | bytes 589828
  83.6 42.7 %collective-permute-start.3 = (bf16[512,384]{1,0:T(8,128)(2,1)}, bf16[512,384]{1,0:T(8,128)(2,1)}, u32[]{:S(2)}, u32[]{:S(2)}) collective-permute-start(bf16[512,384]{1,0:T(8,128)(2,1)} %get-tuple-element.250), channel_id=1, source_target_pairs={{0,248},{8,0},{16,8},{24,16},{32,24},{40,32},{48,40},{56,48},{64,5... | collective-permute-start | bytes 1179656 | tf_op jit(solution)/shard_map/ppermute | solution.py:63
  87.0 40.2 %collective-permute-start.4 = (bf16[512,384]{1,0:T(8,128)(2,1)}, bf16[512,384]{1,0:T(8,128)(2,1)}, u32[]{:S(2)}, u32[]{:S(2)}) collective-permute-start(bf16[512,384]{1,0:T(8,128)(2,1)} %get-tuple-element.249), channel_id=1, source_target_pairs={{0,8},{8,16},{16,24},{24,32},{32,40},{40,48},{48,56},{56,64},{64,7... | collective-permute-start | bytes 1179656 | tf_op jit(solution)/shard_map/ppermute | solution.py:64
  101.3 19.8 %copy-start.5 = (bf16[640,64]{0,1:T(8,128)(2,1)S(1)}, bf16[640,64]{0,1:T(8,128)(2,1)}, u32[]{:S(2)}) copy-start(bf16[640,64]{0,1:T(8,128)(2,1)} %param.29) | copy-start | bytes 245764
  101.3 19.8 %copy-start.6 = (bf16[64,640]{1,0:T(8,128)(2,1)S(1)}, bf16[64,640]{1,0:T(8,128)(2,1)}, u32[]{:S(2)}) copy-start(bf16[64,640]{1,0:T(8,128)(2,1)} %param.28) | copy-start | bytes 245764
  101.3 19.8 %copy-start.7 = (bf16[64,640]{1,0:T(8,128)(2,1)S(1)}, bf16[64,640]{1,0:T(8,128)(2,1)}, u32[]{:S(2)}) copy-start(bf16[64,640]{1,0:T(8,128)(2,1)} %param.27) | copy-start | bytes 245764
  101.3 20.6 %all-to-all-start = ((bf16[2,4,384,256]{3,2,1,0:T(8,128)(2,1)}), bf16[2,4,384,256]{3,2,1,0:T(8,128)(2,1)S(1)}, u32[]{:S(2)}, u32[]{:S(2)}) async-start(bf16[2,4,384,256]{3,2,1,0:T(8,128)(2,1)} %broadcast_in_dim.28), calls=%async_computation | async-start | bytes 3145728 | tf_op jit(solution)/shard_map/all_to_all | solution.py:31
  116.7 126.0 %all-gather.2.cloned.1.call-start = ((), (), s32[]{:S(2)}) async-start(), calls=%async_computation.6 | async-start | bytes 8110080 | tf_op jit(solution)/shard_map/all_gather | solution.py:276
  117.5 15.8 %collective-permute-start = (bf16[1024,256]{1,0:T(8,128)(2,1)}, bf16[1024,256]{1,0:T(8,128)(2,1)S(1)}, u32[]{:S(2)}, u32[]{:S(2)}) collective-permute-start(bf16[1024,256]{1,0:T(8,128)(2,1)} %slice.180), channel_id=1, source_target_pairs={{0,256},{256,0},{1,257},{257,1},{2,258},{258,2},{3,259},{259,3},{4... | collective-permute-start | bytes 1572872 | tf_op jit(solution)/shard_map/ppermute | solution.py:88
  122.0 1.8 copy-start.12
  122.0 1.8 copy-start.13
  122.1 1.3 copy-start
  125.1 13.9 %copy-start.10 = (f32[384]{0:T(512)}, f32[384]{0:T(512)S(1)}, u32[]{:S(2)}) copy-start(f32[384]{0:T(512)S(1)} %add_rsqrt_fusion.1) | copy-start | bytes 4612
  128.5 10.5 %copy-start.1 = (bf16[384,2048]{1,0:T(8,128)(2,1)S(1)}, bf16[384,2048]{1,0:T(8,128)(2,1)}, u32[]{:S(2)}) copy-start(bf16[384,2048]{1,0:T(8,128)(2,1)} %copy-done) | copy-start | bytes 4718596
  128.5 10.5 %copy-start.14 = (f32[2048]{0:T(1024)S(1)}, f32[2048]{0:T(1024)}, u32[]{:S(2)}) copy-start(f32[2048]{0:T(1024)} %param.18) | copy-start | bytes 24580
  133.3 14.0 %collective-permute-start.1 = (bf16[512,256]{1,0:T(8,128)(2,1)S(1)}, bf16[512,256]{1,0:T(8,128)(2,1)S(1)}, u32[]{:S(2)}, u32[]{:S(2)}) collective-permute-start(bf16[512,256]{1,0:T(8,128)(2,1)S(1)} %get-tuple-element.252), channel_id=1, source_target_pairs={{0,248},{8,0},{16,8},{24,16},{32,24},{40,32},{48,40},{56,48},{64,5... | collective-permute-start | bytes 786440 | tf_op jit(solution)/shard_map/ppermute | solution.py:63
  136.5 15.8 %collective-permute-start.2 = (bf16[512,256]{1,0:T(8,128)(2,1)S(1)}, bf16[512,256]{1,0:T(8,128)(2,1)S(1)}, u32[]{:S(2)}, u32[]{:S(2)}) collective-permute-start(bf16[512,256]{1,0:T(8,128)(2,1)S(1)} %get-tuple-element.251), channel_id=1, source_target_pairs={{0,8},{8,16},{16,24},{24,32},{32,40},{40,48},{48,56},{56,64},{64,7... | collective-permute-start | bytes 786440 | tf_op jit(solution)/shard_map/ppermute | solution.py:64
  152.4 0.7 copy-start.11
  153.1 1.0 copy-start.3
  153.1 1.0 copy-start.4
  154.1 0.6 copy-start.9
  203.2 0.7 copy-start.8
Sparse Core Ops, SparseCore 0:
  122.0 120.7 all-gather.1
